TPU v7x, 128 devices: a whole 4x4x4 slice. The times are simulated.
128 devices in a mesh: fs: 32 (over z, y, core), tp: 4 (over x).
Axes of the slice: x: 4, y: 4, z: 4, core: 2. Of those that a mesh axis runs over, the one named last changes fastest.
Arguments:
- x_saved: bfloat16 [65536, 2048], P('fs'), may hold values from -6 to 6
- h_saved: bfloat16 [65536, 1024], P('fs', 'tp'), may hold values from -6 to 6
- key_cot: bfloat16 [65536, 1024], P('fs', 'tp'), may hold values from -6 to 6
- value_cot: bfloat16 [65536, 1024], P('fs', 'tp'), may hold values from -6 to 6
- out_cot: bfloat16 [65536, 2048], P('fs'), may hold values from -6 to 6
- w_key: float32 [2048, 1024], P('fs', 'tp'), may hold values from -0.125 to 0.125
- w_value: float32 [2048, 1024], P('fs', 'tp'), may hold values from -0.125 to 0.125
- w_out: float32 [1024, 2048], P('tp', 'fs'), may hold values from -0.1875 to 0.1875
- p_key: bfloat16 [2048, 256], P('fs'), may hold values from -1 to 1, as said below
- p_value: bfloat16 [2048, 256], P('fs'), may hold values from -1 to 1, as said below
- p_out: bfloat16 [2048, 256], P('fs'), may hold values from -1 to 1, as said below
- m_key: float32 [2, 256, 1024], P(None, 'fs', 'tp'), may hold values from -1.5 to 1.5, as said below
- m_value: float32 [2, 256, 1024], P(None, 'fs', 'tp'), may hold values from -1.5 to 1.5, as said below
- m_out: float32 [2, 256, 1024], P(None, 'fs', 'tp'), may hold values from -1.5 to 1.5, as said below
Outputs:
- step_key: float32 [2048, 1024], P('fs', 'tp')
- step_value: float32 [2048, 1024], P('fs', 'tp')
- step_out: float32 [1024, 2048], P('tp', 'fs')
- copy_key: bfloat16 [2048, 1024], P(None, 'tp')
- copy_value: bfloat16 [2048, 1024], P(None, 'tp')
- copy_out: bfloat16 [1024, 2048], P('tp')
- new_m_key: float32 [2, 256, 1024], P(None, 'fs', 'tp')
- new_m_value: float32 [2, 256, 1024], P(None, 'fs', 'tp')
- new_m_out: float32 [2, 256, 1024], P(None, 'fs', 'tp')
Inputs may be any that keep to these rules, and one draw needn't show every extreme that they name: `p_key`: factor entries are real-valued, dense and of full rank. `p_value`: factor entries are real-valued, dense and of full rank. `p_out`: factor entries are real-valued, dense and of full rank. `m_key`: plane 1 (second moments) lies in 0.05 to 1. `m_value`: plane 1 (second moments) lies in 0.05 to 1. `m_out`: plane 1 (second moments) lies in 0.05 to 1.
All inputs are finite; a program needn't handle non-finite values.
Results may differ from a plain program's by a relative error of at most 0.0085.
Values may be sent and summed in bfloat16 or wider, within the bound.
No kernel may reach another device: no remote copies, remote signals or barrier semaphores. Data moves between devices by JAX's collectives and lax.ppermute only.
A program may use at most 128 MiB of HBM per device.

v0:
```python
import jax
import jax.numpy as jnp
from jax import lax
from jax.sharding import Mesh
from jax.sharding import PartitionSpec as P

FS = ("fs_0", "fs_1", "fs_2")


beta_one = 0.9
beta_two = 0.9
learn_rate = 0.01


def copy_for_each(value, axis):
    copies = jnp.broadcast_to(value, (lax.axis_size(axis), *value.shape))
    return lax.all_to_all(copies, axis, split_axis=0, concat_axis=0, tiled=True)


def joined_along(parts, dim):
    parts = jnp.moveaxis(parts, 0, dim)
    dims = parts.shape
    return parts.reshape(*dims[:dim], dims[dim] * dims[dim + 1], *dims[dim + 2 :])


def whole_of(value, axes, dim):
    far, near = axes
    first = copy_for_each(value, far)
    parts = jnp.swapaxes(copy_for_each(first, near), 0, 1)
    return joined_along(parts.reshape(-1, *value.shape), dim)


def in_one_piece(arrays, axis, dim, along):
    widths = [a.shape[along] for a in arrays]
    both = jnp.concatenate(arrays, axis=along)
    whole = whole_of(both, axis, dim)
    return tuple(jnp.split(whole, [sum(widths[:k]) for k in range(1, len(widths))], axis=along))


def in_blocks(value, dim, devices):
    dims = value.shape
    parts = value.reshape(*dims[:dim], devices, dims[dim] // devices, *dims[dim + 1 :])
    return jnp.moveaxis(parts, dim, 0)


def sent_and_summed(value, axis, dim):
    devices = lax.axis_size(axis)
    parts = lax.all_to_all(in_blocks(value, dim, devices), axis, 0, 0, tiled=True)
    return jnp.sum(parts.astype(jnp.float32), axis=0)


def over_copies(value, axis):
    return copy_for_each(value, axis).sum(axis=0)


def over_axes(value, axes):
    far, near = axes
    return over_copies(over_copies(value, near), far)


def gathered_copies(value, axis, dim):
    return joined_along(copy_for_each(value, axis), dim)


def project_rows(factors, grads, local_width):
    high_part = grads.astype(jnp.bfloat16)
    low_part = (grads - high_part.astype(jnp.float32)).astype(jnp.bfloat16)
    outputs = []
    for member in range(3):
        lower = member * local_width
        upper = (member + 1) * local_width
        factor_t = factors[member].T
        first_term = jnp.dot(
            factor_t, high_part[:, lower:upper], preferred_element_type=jnp.float32
        )
        second_term = jnp.dot(
            factor_t, low_part[:, lower:upper], preferred_element_type=jnp.float32
        )
        outputs.append(first_term + second_term)
    return jnp.concatenate(outputs, axis=1)


def body(
    x_saved,
    h_saved,
    key_cot,
    value_cot,
    out_cot,
    w_key,
    w_value,
    w_out,
    p_key,
    p_value,
    p_out,
    m_key,
    m_value,
    m_out,
):
    local_width = key_cot.shape[1]
    x_cols = x_saved.T
    y_cols = out_cot.T
    grad_k = jnp.dot(x_cols, key_cot, preferred_element_type=jnp.float32)
    grad_v = jnp.dot(x_cols, value_cot, preferred_element_type=jnp.float32)
    grad_o = jnp.dot(y_cols, h_saved, preferred_element_type=jnp.float32)
    whole_grad = jnp.concatenate([grad_k, grad_v, grad_o], axis=1)
    partial_value = project_rows(
        in_one_piece((p_key, p_value, p_out), (("fs_0", "fs_1"), "fs_2"), 0, 1),
        whole_grad,
        local_width,
    )
    projected = sent_and_summed(partial_value.astype(jnp.bfloat16), FS, 0)
    total = over_axes(jnp.sum(projected * projected), (("fs_0", "fs_1"), ("fs_2", "tp")))
    entries = projected.size * lax.axis_size(FS) * lax.axis_size("tp")
    normed = projected / jnp.sqrt(total / entries + 1e-06)
    moments = jnp.concatenate([m_key, m_value, m_out], axis=2)
    moment_one = beta_one * moments[0] + (1 - beta_one) * normed
    moment_two = beta_two * moments[1] + (1 - beta_two) * normed * normed
    direction = (moment_one / jnp.sqrt(moment_two)).astype(jnp.bfloat16)
    gathered = gathered_copies(direction, FS, 0)
    step_key = jnp.dot(p_key, gathered[:, :local_width], preferred_element_type=jnp.float32)
    step_value = jnp.dot(
        p_value, gathered[:, local_width : 2 * local_width], preferred_element_type=jnp.float32
    )
    step_out = jnp.dot(p_out, gathered[:, 2 * local_width :], preferred_element_type=jnp.float32).T
    fresh_key = (w_key - learn_rate * step_key).astype(jnp.bfloat16)
    fresh_value = (w_value - learn_rate * step_value).astype(jnp.bfloat16)
    fresh_out = (w_out - learn_rate * step_out).astype(jnp.bfloat16)
    copy_key, copy_value, copy_out = (
        *in_one_piece((fresh_key, fresh_value), (("fs_0", "fs_1"), "fs_2"), 0, 1),
        whole_of(fresh_out, (("fs_0", "fs_1"), "fs_2"), 1),
    )
    stacked = jnp.stack([moment_one, moment_two])
    new_m_key = stacked[:, :, :local_width]
    new_m_value = stacked[:, :, local_width : 2 * local_width]
    new_m_out = stacked[:, :, 2 * local_width :]
    return (
        step_key,
        step_value,
        step_out,
        copy_key,
        copy_value,
        copy_out,
        new_m_key,
        new_m_value,
        new_m_out,
    )


def solution(mesh):
    split = Mesh(mesh.devices.reshape(4, 4, 2, mesh.shape["tp"]), ("fs_0", "fs_1", "fs_2", "tp"))
    in_specs = (
        P(FS, None),
        P(FS, "tp"),
        P(FS, "tp"),
        P(FS, "tp"),
        P(FS, None),
        P(FS, "tp"),
        P(FS, "tp"),
        P("tp", FS),
        P(FS, None),
        P(FS, None),
        P(FS, None),
        P(None, FS, "tp"),
        P(None, FS, "tp"),
        P(None, FS, "tp"),
    )
    out_specs = (
        P(FS, "tp"),
        P(FS, "tp"),
        P("tp", FS),
        P(None, "tp"),
        P(None, "tp"),
        P("tp", None),
        P(None, FS, "tp"),
        P(None, FS, "tp"),
        P(None, FS, "tp"),
    )
    return jax.shard_map(body, mesh=split, in_specs=in_specs, out_specs=out_specs, check_vma=False)
```

profile of v0, /device:TPU:1, one launch (start us, length us, event | category | flops | bytes accessed | tf_op | source)
XLA Modules:
  0.0 154.7 jit_solution(2395847541230072677)
XLA Ops:
  0.6 0.0 copy-start
  0.7 0.9 pad_maximum_fusion.2
  1.5 1.3 broadcast_in_dim.27
  2.9 8.6 %all-to-all-start = ((bf16[16,64,768]{2,1,0:T(8,128)(2,1)}), bf16[16,64,768]{2,1,0:T(8,128)(2,1)S(1)}, u32[]{:S(2)}, u32[]{:S(2)}) async-start(bf16[16,64,768]{2,1,0:T(8,128)(2,1)} %broadcast_in_dim.27), calls=%async_computation | async-start | bytes 3145728 | tf_op jit(solution)/shard_map/all_to_all | solution.py:17
  11.5 0.0 copy-start.12
  11.5 0.0 slice-start
  11.5 5.9 %fusion.34 = f32[2048,256]{0,1:T(8,128)S(1)} fusion(bf16[2048,2048]{1,0:T(8,128)(2,1)} %param.14, bf16[2048,256]{1,0:T(8,128)(2,1)S(1)} %copy-done), kind=kOutput, calls=%fused_computation.64 | convolution fusion | flops 2147483648 | bytes 11534336 | tf_op jit(solution)/shard_map/dot_general | solution.py:102
  17.4 0.0 slice-start.1
  17.4 0.0 copy-start.13
  17.4 5.9 %fusion.35 = f32[2048,256]{0,1:T(8,128)S(1)} fusion(bf16[2048,2048]{1,0:T(8,128)(2,1)} %param.14, bf16[2048,256]{1,0:T(8,128)(2,1)S(1)} %copy-done.12), kind=kOutput, calls=%fused_computation.65 | convolution fusion | flops 2147483648 | bytes 11534336 | tf_op jit(solution)/shard_map/dot_general | solution.py:103
  23.4 2.4 %fusion.36 = f32[2048,256]{0,1:T(8,128)S(1)} fusion(bf16[2048,2048]{1,0:T(8,128)(2,1)S(1)} %bitcast.52, bf16[2048,256]{1,0:T(8,128)(2,1)S(1)} %copy-done.13), kind=kOutput, calls=%fused_computation.66 | convolution fusion | flops 2147483648 | bytes 11534336 | tf_op jit(solution)/shard_map/dot_general | solution.py:104
  25.8 2.1 %subtract_convert_fusion = bf16[2048,768]{0,1:T(8,128)(2,1)} fusion(f32[2048,256]{0,1:T(8,128)S(1)} %fusion.36, f32[2048,256]{0,1:T(8,128)S(1)} %fusion.35, f32[2048,256]{0,1:T(8,128)S(1)} %fusion.34), kind=kLoop, calls=%fused_computation.1 | loop fusion | flops 9437184 | bytes 9437184 | tf_op jit(solution)/shard_map/convert_element_type | solution.py:67
  27.8 2.0 %fusion = bf16[2048,768]{0,1:T(8,128)(2,1)} fusion(f32[2048,256]{0,1:T(8,128)S(1)} %fusion.36, f32[2048,256]{0,1:T(8,128)S(1)} %fusion.35, f32[2048,256]{0,1:T(8,128)S(1)} %fusion.34), kind=kLoop, calls=%fused_computation.2 | loop fusion | flops 9437184 | bytes 9437184 | tf_op jit(solution)/shard_map/convert_element_type | solution.py:66
  29.8 4.7 %all-to-all-done = bf16[16,64,768]{2,1,0:T(8,128)(2,1)S(1)} async-done(((bf16[16,64,768]{2,1,0:T(8,128)(2,1)}), bf16[16,64,768]{2,1,0:T(8,128)(2,1)S(1)}, u32[]{:S(2)}, u32[]{:S(2)}) %all-to-all-start) | async-done | bytes 1572896 | tf_op jit(solution)/shard_map/all_to_all | solution.py:17
  34.5 0.4 broadcast_in_dim.28
  35.0 8.3 %all_to_all.52 = bf16[2,16,64,768]{3,2,1,0:T(8,128)(2,1)S(1)} all-to-all(bf16[2,16,64,768]{3,2,1,0:T(8,128)(2,1)S(1)} %broadcast_in_dim.28), channel_id=1, replica_groups=mesh['fs_0'=4,'fs_1'=4,'fs_2'=2,'tp'=4] {'fs_2'}, dimensions={0} | all-to-all | bytes 6291456 | tf_op jit(solution)/shard_map/all_to_all | solution.py:17
  43.2 0.3 copy.36
  43.6 1.6 %copy-done.2 = bf16[2048,768]{0,1:T(8,128)(2,1)S(1)} copy-done((bf16[2048,768]{0,1:T(8,128)(2,1)S(1)}, bf16[2048,768]{0,1:T(8,128)(2,1)}, u32[]{:S(2)}) %copy-start.2) | copy-done | bytes 3145752
  45.1 0.5 fusion.11
  45.6 0.5 fusion.8
  46.1 0.5 fusion.14
  46.6 0.9 copy-done.1
  47.5 0.5 fusion.5
  48.0 0.5 fusion.6
  48.5 0.0 copy-start.9
  48.5 0.0 copy-start.10
  48.5 0.0 copy-start.11
  48.5 0.0 copy-start.3
  48.5 0.0 copy-start.6
  48.5 0.5 fusion.4
  49.0 0.0 copy-start.4
  49.0 0.0 copy-start.7
  49.1 0.0 copy-start.5
  49.1 0.8 pad_maximum_fusion.1
  49.9 3.9 %all-to-all-start.2 = ((bf16[32,8,768]{2,1,0:T(8,128)(2,1)}), bf16[32,8,768]{2,1,0:T(8,128)(2,1)S(1)}, u32[]{:S(2)}, u32[]{:S(2)}) async-start(bf16[32,8,768]{2,1,0:T(8,128)(2,1)} %pad_maximum_fusion.1), calls=%async_computation.2 | async-start | bytes 786432 | tf_op jit(solution)/shard_map/all_to_all | solution.py:48
  53.8 10.2 %all-to-all-done.2 = bf16[32,8,768]{2,1,0:T(8,128)(2,1)S(1)} async-done(((bf16[32,8,768]{2,1,0:T(8,128)(2,1)}), bf16[32,8,768]{2,1,0:T(8,128)(2,1)S(1)}, u32[]{:S(2)}, u32[]{:S(2)}) %all-to-all-start.2) | async-done | bytes 393248 | tf_op jit(solution)/shard_map/all_to_all | solution.py:48
  64.0 0.1 convert_reduce_fusion
  64.1 0.6 multiply_reduce_fusion
  64.7 0.6 broadcast_in_dim.29
  65.3 9.0 %all_to_all.53 = f32[8,1,1]{2,1,0:T(1,128)S(1)} all-to-all(f32[8,1,1]{2,1,0:T(1,128)S(1)} %broadcast_in_dim.29), channel_id=1, replica_groups=mesh['fs_0'=4,'fs_1'=4,'fs_2'=2,'tp'=4] {'fs_2','tp'}, dimensions={0} | all-to-all | bytes 64 | tf_op jit(solution)/shard_map/all_to_all | solution.py:17
  74.3 0.6 reduce_sum.38
  74.9 1.2 broadcast_in_dim.30
  76.2 3.5 %all-to-all-start.4 = ((f32[16,1,1]{2,1,0:T(1,128)}), f32[16,1,1]{2,1,0:T(1,128)S(1)}, u32[]{:S(2)}, u32[]{:S(2)}) async-start(f32[16,1,1]{2,1,0:T(1,128)} %broadcast_in_dim.30), calls=%async_computation.4 | async-start | bytes 16384 | tf_op jit(solution)/shard_map/all_to_all | solution.py:17
  79.7 6.3 %all-to-all-done.4 = f32[16,1,1]{2,1,0:T(1,128)S(1)} async-done(((f32[16,1,1]{2,1,0:T(1,128)}), f32[16,1,1]{2,1,0:T(1,128)S(1)}, u32[]{:S(2)}, u32[]{:S(2)}) %all-to-all-start.4) | async-done | bytes 96 | tf_op jit(solution)/shard_map/all_to_all | solution.py:17
  86.0 0.6 reduce_sum.39
  87.3 15.0 %all_to_all.54 = bf16[32,8,768]{2,1,0:T(8,128)(2,1)S(1)} all-to-all(bf16[32,8,768]{2,1,0:T(8,128)(2,1)S(1)} %broadcast_in_dim.31), channel_id=1, replica_groups=mesh['fs_0'=4,'fs_1'=4,'fs_2'=2,'tp'=4] {'fs_0','fs_1','fs_2'}, dimensions={0} | all-to-all | bytes 786432 | tf_op jit(solution)/shard_map/all_to_all | solution.py:17
  102.4 0.8 subtract_convert_fusion.1
  103.2 0.8 broadcast_in_dim.34
  104.0 3.6 %all-to-all-start.8 = ((bf16[16,256,64]{1,2,0:T(8,128)(2,1)}), bf16[16,256,64]{1,2,0:T(8,128)(2,1)S(1)}, u32[]{:S(2)}, u32[]{:S(2)}) async-start(bf16[16,256,64]{1,2,0:T(8,128)(2,1)} %broadcast_in_dim.34), calls=%async_computation.8 | async-start | bytes 1048576 | tf_op jit(solution)/shard_map/all_to_all | solution.py:17
  107.6 0.8 subtract_convert_fusion.2
  108.4 0.8 subtract_convert_fusion.3
  109.2 9.4 %all-to-all-done.8 = bf16[16,256,64]{1,2,0:T(8,128)(2,1)S(1)} async-done(((bf16[16,256,64]{1,2,0:T(8,128)(2,1)}), bf16[16,256,64]{1,2,0:T(8,128)(2,1)S(1)}, u32[]{:S(2)}, u32[]{:S(2)}) %all-to-all-start.8) | async-done | bytes 524320 | tf_op jit(solution)/shard_map/all_to_all | solution.py:17
  118.6 0.1 broadcast_in_dim.35
  118.7 5.6 %all_to_all.55 = bf16[2,16,256,64]{2,3,1,0:T(8,128)(2,1)S(1)} all-to-all(bf16[2,16,256,64]{2,3,1,0:T(8,128)(2,1)S(1)} %broadcast_in_dim.35), channel_id=1, replica_groups=mesh['fs_0'=4,'fs_1'=4,'fs_2'=2,'tp'=4] {'fs_2'}, dimensions={0} | all-to-all | bytes 2097152 | tf_op jit(solution)/shard_map/all_to_all | solution.py:17
  124.4 1.1 broadcast_in_dim.32
  125.4 3.7 %all-to-all-start.6 = ((bf16[16,64,512]{2,1,0:T(8,128)(2,1)}), bf16[16,64,512]{2,1,0:T(8,128)(2,1)S(1)}, u32[]{:S(2)}, u32[]{:S(2)}) async-start(bf16[16,64,512]{2,1,0:T(8,128)(2,1)} %broadcast_in_dim.32), calls=%async_computation.6 | async-start | bytes 2097152 | tf_op jit(solution)/shard_map/all_to_all | solution.py:17
  129.1 0.6 pad_maximum_fusion.4
  129.7 1.0 copy.40
  130.8 2.3 %copy.41 = bf16[256,2048]{1,0:T(8,128)(2,1)} copy(bf16[256,2048]{0,1:T(8,128)(2,1)} %bitcast.41) | data formatting | bytes 2097152
  133.0 12.9 %all-to-all-done.6 = bf16[16,64,512]{2,1,0:T(8,128)(2,1)S(1)} async-done(((bf16[16,64,512]{2,1,0:T(8,128)(2,1)}), bf16[16,64,512]{2,1,0:T(8,128)(2,1)S(1)}, u32[]{:S(2)}, u32[]{:S(2)}) %all-to-all-start.6) | async-done | bytes 1048608 | tf_op jit(solution)/shard_map/all_to_all | solution.py:17
  146.0 0.2 broadcast_in_dim.33
  146.2 6.9 %all_to_all.56 = bf16[2,16,64,512]{3,2,1,0:T(8,128)(2,1)S(1)} all-to-all(bf16[2,16,64,512]{3,2,1,0:T(8,128)(2,1)S(1)} %broadcast_in_dim.33), channel_id=1, replica_groups=mesh['fs_0'=4,'fs_1'=4,'fs_2'=2,'tp'=4] {'fs_2'}, dimensions={0} | all-to-all | bytes 4194304 | tf_op jit(solution)/shard_map/all_to_all | solution.py:17
  153.1 0.2 copy.39
  153.3 1.5 fusion.33
  (25 shorter events, 0.1 us)
Async XLA Ops:
  0.6 10.8 %copy-start = (bf16[2048,256]{1,0:T(8,128)(2,1)S(1)}, bf16[2048,256]{1,0:T(8,128)(2,1)}, u32[]{:S(2)}) copy-start(bf16[2048,256]{1,0:T(8,128)(2,1)} %param.16) | copy-start | bytes 3145732
  2.9 31.7 %all-to-all-start = ((bf16[16,64,768]{2,1,0:T(8,128)(2,1)}), bf16[16,64,768]{2,1,0:T(8,128)(2,1)S(1)}, u32[]{:S(2)}, u32[]{:S(2)}) async-start(bf16[16,64,768]{2,1,0:T(8,128)(2,1)} %broadcast_in_dim.27), calls=%async_computation | async-start | bytes 3145728 | tf_op jit(solution)/shard_map/all_to_all | solution.py:17
  11.5 5.9 %copy-start.12 = (bf16[2048,256]{1,0:T(8,128)(2,1)S(1)}, bf16[2048,256]{1,0:T(8,128)(2,1)}, u32[]{:S(2)}) copy-start(bf16[2048,256]{1,0:T(8,128)(2,1)} %param.17) | copy-start | bytes 3145732
  11.5 11.9 %slice-start = ((s8[8388608]{0:T(1024)(128)(4,1)}), s8[4194304]{0:T(1024)(128)(4,1)S(1)}, s32[]{:S(2)}) async-start(s8[8388608]{0:T(1024)(128)(4,1)} %bitcast.51), calls=%async_computation.10 | async-start | bytes 8388608
  17.4 5.9 %slice-start.1 = ((s8[8388608]{0:T(1024)(128)(4,1)}), s8[4194304]{0:T(1024)(128)(4,1)S(1)}, s32[]{:S(2)}) async-start(s8[8388608]{0:T(1024)(128)(4,1)} %bitcast.51), calls=%async_computation.11 | async-start | bytes 8388608
  17.4 5.9 %copy-start.13 = (bf16[2048,256]{1,0:T(8,128)(2,1)S(1)}, bf16[2048,256]{1,0:T(8,128)(2,1)}, u32[]{:S(2)}) copy-start(bf16[2048,256]{1,0:T(8,128)(2,1)} %param.15) | copy-start | bytes 3145732
  43.2 1.9 %copy-start.2 = (bf16[2048,768]{0,1:T(8,128)(2,1)S(1)}, bf16[2048,768]{0,1:T(8,128)(2,1)}, u32[]{:S(2)}) copy-start(bf16[2048,768]{0,1:T(8,128)(2,1)} %fusion) | copy-start | bytes 9437188
  45.6 1.9 %copy-start.1 = (bf16[2048,768]{0,1:T(8,128)(2,1)S(1)}, bf16[2048,768]{0,1:T(8,128)(2,1)}, u32[]{:S(2)}) copy-start(bf16[2048,768]{0,1:T(8,128)(2,1)} %subtract_convert_fusion) | copy-start | bytes 9437188
  48.5 5.3 %copy-start.9 = (f32[2,8,256]{2,1,0:T(8,128)S(1)}, f32[2,8,256]{2,1,0:T(8,128)}, u32[]{:S(2)}) copy-start(f32[2,8,256]{2,1,0:T(8,128)} %param.25) | copy-start | bytes 49156
  48.5 5.3 %copy-start.10 = (f32[2,8,256]{2,1,0:T(8,128)S(1)}, f32[2,8,256]{2,1,0:T(8,128)}, u32[]{:S(2)}) copy-start(f32[2,8,256]{2,1,0:T(8,128)} %param.26) | copy-start | bytes 49156
  48.5 31.2 %copy-start.11 = (f32[2,8,256]{2,1,0:T(8,128)S(1)}, f32[2,8,256]{2,1,0:T(8,128)}, u32[]{:S(2)}) copy-start(f32[2,8,256]{2,1,0:T(8,128)} %param.27) | copy-start | bytes 49156
  48.5 53.9 %copy-start.3 = (bf16[64,256]{1,0:T(8,128)(2,1)S(1)}, bf16[64,256]{1,0:T(8,128)(2,1)}, u32[]{:S(2)}) copy-start(bf16[64,256]{1,0:T(8,128)(2,1)} %param.24) | copy-start | bytes 98308
  48.5 53.8 %copy-start.6 = (f32[256,64]{0,1:T(8,128)S(1)}, f32[256,64]{0,1:T(8,128)}, u32[]{:S(2)}) copy-start(f32[256,64]{0,1:T(8,128)} %param.21) | copy-start | bytes 196612
  49.0 58.6 %copy-start.4 = (bf16[64,256]{1,0:T(8,128)(2,1)S(1)}, bf16[64,256]{1,0:T(8,128)(2,1)}, u32[]{:S(2)}) copy-start(bf16[64,256]{1,0:T(8,128)(2,1)} %param.23) | copy-start | bytes 98308
  49.0 58.6 %copy-start.7 = (f32[64,256]{1,0:T(8,128)S(1)}, f32[64,256]{1,0:T(8,128)}, u32[]{:S(2)}) copy-start(f32[64,256]{1,0:T(8,128)} %param.20) | copy-start | bytes 196612
  49.1 59.3 %copy-start.5 = (bf16[64,256]{1,0:T(8,128)(2,1)S(1)}, bf16[64,256]{1,0:T(8,128)(2,1)}, u32[]{:S(2)}) copy-start(bf16[64,256]{1,0:T(8,128)(2,1)} %param.22) | copy-start | bytes 98308
  49.1 59.3 %copy-start.8 = (f32[64,256]{1,0:T(8,128)S(1)}, f32[64,256]{1,0:T(8,128)}, u32[]{:S(2)}) copy-start(f32[64,256]{1,0:T(8,128)} %param.19) | copy-start | bytes 196612
  49.9 14.2 %all-to-all-start.2 = ((bf16[32,8,768]{2,1,0:T(8,128)(2,1)}), bf16[32,8,768]{2,1,0:T(8,128)(2,1)S(1)}, u32[]{:S(2)}, u32[]{:S(2)}) async-start(bf16[32,8,768]{2,1,0:T(8,128)(2,1)} %pad_maximum_fusion.1), calls=%async_computation.2 | async-start | bytes 786432 | tf_op jit(solution)/shard_map/all_to_all | solution.py:48
  76.2 9.8 %all-to-all-start.4 = ((f32[16,1,1]{2,1,0:T(1,128)}), f32[16,1,1]{2,1,0:T(1,128)S(1)}, u32[]{:S(2)}, u32[]{:S(2)}) async-start(f32[16,1,1]{2,1,0:T(1,128)} %broadcast_in_dim.30), calls=%async_computation.4 | async-start | bytes 16384 | tf_op jit(solution)/shard_map/all_to_all | solution.py:17
  104.0 14.6 %all-to-all-start.8 = ((bf16[16,256,64]{1,2,0:T(8,128)(2,1)}), bf16[16,256,64]{1,2,0:T(8,128)(2,1)S(1)}, u32[]{:S(2)}, u32[]{:S(2)}) async-start(bf16[16,256,64]{1,2,0:T(8,128)(2,1)} %broadcast_in_dim.34), calls=%async_computation.8 | async-start | bytes 1048576 | tf_op jit(solution)/shard_map/all_to_all | solution.py:17
  125.4 20.5 %all-to-all-start.6 = ((bf16[16,64,512]{2,1,0:T(8,128)(2,1)}), bf16[16,64,512]{2,1,0:T(8,128)(2,1)S(1)}, u32[]{:S(2)}, u32[]{:S(2)}) async-start(bf16[16,64,512]{2,1,0:T(8,128)(2,1)} %broadcast_in_dim.32), calls=%async_computation.6 | async-start | bytes 2097152 | tf_op jit(solution)/shard_map/all_to_all | solution.py:17
where the time goes:
time: 156 us; the launch traced here: 155 us
  blocking collectives  44.8 us (29%)
  waiting for transfers between devices  43.5 us (28%)
  starting transfers between devices  23.2 us (15%)
  matrix products  19.4 us (12%)
  local copies, waits for them, and re-layouts  13.8 us (9%)
  other arithmetic  8.29 us (5%)
  between operations  1.75 us (1%)
    all_to_all x5, blocking collectives, copy_for_each(): return lax.all_to_all(copies, axis, split_axis=0, concat_axis=0, tiled=True)  44.8 us
    all_to_all x4, waiting for transfers between devices, copy_for_each(): return lax.all_to_all(copies, axis, split_axis=0, concat_axis=0, tiled=True)  33.3 us
    all_to_all x4, starting transfers between devices, copy_for_each(): return lax.all_to_all(copies, axis, split_axis=0, concat_axis=0, tiled=True)  19.3 us
    all_to_all x1, waiting for transfers between devices, sent_and_summed(): lax.all_to_all(in_blocks(value, dim, devices), axis, 0, 0, tiled=True)  10.2 us
    broadcast_in_dim x9, local copies, waits for them, and re-layouts, copy_for_each(): copies = jnp.broadcast_to(value, (lax.axis_size(axis), *value.shape))  5.9 us
    dot_general x1, matrix products, body(): grad_k = jnp.dot(x_cols, key_cot, preferred_element_type=jnp.float32)  5.9 us
    dot_general x1, matrix products, body(): grad_v = jnp.dot(x_cols, value_cot, preferred_element_type=jnp.float32)  5.9 us
    unnamed x35, local copies, waits for them, and re-layouts  4.84 us
  transfers between devices with their start and end apart: 5, of which 5 were waited for; matrix products, arithmetic and copies ran while one was open for 15% of the time, Pallas kernels for 0%

commit v1 on v0

v1 whole, which is shorter than its diff:
```python
import jax
import jax.numpy as jnp
from jax import lax
from jax.experimental import pallas as pl
from jax.experimental.pallas import tpu as pltpu
from jax.sharding import Mesh
from jax.sharding import PartitionSpec as P

FS = ("fs_0", "fs_1", "fs_2")
FAR = ("fs_0", "fs_1")
CORE = "fs_2"
MIB = 1024 * 1024

beta_one = 0.9
beta_two = 0.9
learn_rate = 0.01


def vmem():
    return pl.BlockSpec(memory_space=pltpu.VMEM)


def smem():
    return pl.BlockSpec(memory_space=pltpu.SMEM)


def shift(value, axis, by):
    size = lax.axis_size(axis)
    return lax.ppermute(value, axis, [(i, (i + by) % size) for i in range(size)])


def mirrored(value, axis, by):
    size = lax.axis_size(axis)
    pairs = []
    for place in range(size):
        pairs.append((place * 2, (place + by) % size * 2))
        pairs.append((place * 2 + 1, (place - by) % size * 2 + 1))
    return lax.ppermute(value, (axis, CORE), pairs)


def swap(value):
    return shift(value, CORE, 1)


def spread_kernel(a_ref, b_ref, c_ref, out_ref):
    for copy in range(16):
        for member, ref in enumerate((a_ref, b_ref, c_ref)):
            out_ref[copy, :, pl.ds(member * 256, 256)] = ref[...]


def spread(a, b, c):
    return pl.pallas_call(
        spread_kernel,
        out_shape=jax.ShapeDtypeStruct((16, 64, 768), jnp.bfloat16),
        in_specs=[vmem()] * 3,
        out_specs=vmem(),
        name="spread",
    )(a, b, c)


def split_lanes(grad, first, keep_ref, send_ref, rows, start):
    for pair in range(grad.shape[1] // 256):
        left = grad[:, pair * 256 : pair * 256 + 128]
        right = grad[:, pair * 256 + 128 : pair * 256 + 256]
        low_half = lax.broadcasted_iota(jnp.int32, left.shape, 1) < 64
        turned = pltpu.roll(jnp.where(low_half, right, left), 64, 1)
        zero = jnp.where(low_half, left, turned)
        one = jnp.where(low_half, turned, right)
        columns = pl.ds(start + pair * 128, 128)
        keep_ref[rows, columns] = jnp.where(first, zero, one)
        send_ref[rows, columns] = jnp.where(first, one, zero).astype(jnp.bfloat16)


TILE = 1024
TILES = 2048 // TILE


def grad_kernel(
    core_ref,
    k_ref,
    v_ref,
    h_ref,
    x_ref,
    o_ref,
    keep_ref,
    send_ref,
    narrow_ref,
    wide_ref,
    keep_buf,
    send_buf,
    narrow_sem,
    wide_sem,
    out_sem,
):
    narrow = [
        pltpu.make_async_copy(ref, narrow_ref.at[n], narrow_sem.at[n])
        for n, ref in enumerate((k_ref, v_ref, h_ref))
    ]
    wide = [
        pltpu.make_async_copy(
            ref.at[:, pl.ds(tile * TILE, TILE)],
            wide_ref.at[group, :, pl.ds(tile * TILE, TILE)],
            wide_sem.at[group * TILES + tile],
        )
        for group, ref in enumerate((x_ref, o_ref))
        for tile in range(TILES)
    ]
    narrow[0].start()
    wide[0].start()
    narrow[1].start()
    for copy in wide[1:TILES]:
        copy.start()
    narrow[2].start()
    for copy in wide[TILES:]:
        copy.start()
    first = core_ref[0] == 0
    outs = []
    for group, members in enumerate(((0, 1), (2,))):
        for tile in range(TILES):
            if tile == 0:
                narrow[members[0]].wait()
            wide[group * TILES + tile].wait()
            for member in members:
                if tile == 0 and member == 1:
                    narrow[1].wait()
                rows = pl.ds(member * 256, 256)
                grad = lax.dot_general(
                    narrow_ref[member],
                    wide_ref[group, :, pl.ds(tile * TILE, TILE)],
                    (((0,), (0,)), ((), ())),
                    preferred_element_type=jnp.float32,
                )
                split_lanes(grad, first, keep_buf, send_buf, rows, tile * TILE // 2)
        rows = pl.ds(members[0] * 256, len(members) * 256)
        for side, (buf, ref) in enumerate(((keep_buf, keep_ref), (send_buf, send_ref))):
            copy = pltpu.make_async_copy(
                buf.at[rows, :], ref.at[rows, :], out_sem.at[group * 2 + side]
            )
            copy.start()
            outs.append(copy)
    for copy in outs:
        copy.wait()


def hbm_only(value):
    return pltpu.with_memory_space_constraint(value, pltpu.HBM)


def in_hbm():
    return pl.BlockSpec(memory_space=pltpu.HBM)


def grad_halves(core, key_cot, value_cot, h_saved, x_saved, out_cot):
    return pl.pallas_call(
        grad_kernel,
        out_shape=(
            pltpu.HBM((768, 1024), jnp.float32),
            pltpu.HBM((768, 1024), jnp.bfloat16),
        ),
        in_specs=[smem()] + [in_hbm()] * 5,
        out_specs=(in_hbm(), in_hbm()),
        scratch_shapes=[
            pltpu.VMEM((3, 2048, 256), jnp.bfloat16),
            pltpu.VMEM((2, 2048, 2048), jnp.bfloat16),
            pltpu.VMEM((768, 1024), jnp.float32),
            pltpu.VMEM((768, 1024), jnp.bfloat16),
            pltpu.SemaphoreType.DMA((3,)),
            pltpu.SemaphoreType.DMA((2 * TILES,)),
            pltpu.SemaphoreType.DMA((4,)),
        ],
        compiler_params=pltpu.CompilerParams(vmem_limit_bytes=48 * MIB),
        name="grads",
    )(core, *[hbm_only(a) for a in (key_cot, value_cot, h_saved, x_saved, out_cot)])


def pair_kernel(keep_ref, recv_ref, parts_ref, keep_buf, sem):
    copies = []
    for member in range(3):
        rows = pl.ds(member * 256, 256)
        copies.append(
            pltpu.make_async_copy(keep_ref.at[rows, :], keep_buf.at[rows, :], sem.at[member])
        )
        copies[member].start()
    for member in range(3):
        rows = pl.ds(member * 256, 256)
        copies[member].wait()
        grad = keep_buf[rows, :] + recv_ref[rows, :].astype(jnp.float32)
        parts_ref[member] = grad.astype(jnp.bfloat16)


def pair_sum(keep, recv):
    return pl.pallas_call(
        pair_kernel,
        out_shape=jax.ShapeDtypeStruct((3, 256, 1024), jnp.bfloat16),
        in_specs=[in_hbm(), vmem()],
        out_specs=vmem(),
        scratch_shapes=[
            pltpu.VMEM((768, 1024), jnp.float32),
            pltpu.SemaphoreType.DMA((3,)),
        ],
        compiler_params=pltpu.CompilerParams(vmem_limit_bytes=12 * MIB),
        name="pair_sum",
    )(hbm_only(keep), recv)


def project_kernel(parts_ref, p_ref, out_ref):
    tiles = []
    for member in range(3):
        both = jnp.dot(
            parts_ref[member],
            p_ref[:, pl.ds(member * 256, 256)],
            preferred_element_type=jnp.float32,
        )
        turned = both.T
        for lanes in range(2):
            tiles.append(turned[:, lanes * 128 : (lanes + 1) * 128].reshape(32, 8, 128))
    upper = lax.broadcasted_iota(jnp.int32, (32, 8, 128), 1) < 4
    for half in range(2):
        one, two, shared = tiles[3 * half : 3 * half + 3]
        for side, whole in enumerate((one, two)):
            part = shared if side == 0 else pltpu.roll(shared, 4, 1)
            piece = jnp.concatenate([whole, jnp.where(upper, part, 0.0)], axis=1)
            out_ref[:, 2 * half + side] = piece.astype(jnp.bfloat16)


def project(parts, factors):
    return pl.pallas_call(
        project_kernel,
        out_shape=jax.ShapeDtypeStruct((32, 4, 16, 128), jnp.bfloat16),
        in_specs=[vmem(), vmem()],
        out_specs=vmem(),
        compiler_params=pltpu.CompilerParams(vmem_limit_bytes=12 * MIB),
        name="project",
    )(parts, factors)


def reduce_kernel(pieces_ref, out_ref):
    own = jnp.sum(pieces_ref[...].astype(jnp.float32), axis=0)
    total = jnp.sum(own * own)
    high = total.astype(jnp.bfloat16).astype(jnp.float32)
    row = lax.broadcasted_iota(jnp.int32, own.shape, 1)
    lane = lax.broadcasted_iota(jnp.int32, own.shape, 2)
    tail = jnp.where(row == 12, high, total - high)
    value = jnp.where(row < 12, own, jnp.where((lane == 0) & (row < 14), tail, 0.0))
    out_ref[...] = jnp.broadcast_to(value.astype(jnp.bfloat16)[None], out_ref.shape)


def reduce_pieces(pieces):
    return pl.pallas_call(
        reduce_kernel,
        out_shape=jax.ShapeDtypeStruct((32, 4, 16, 128), jnp.bfloat16),
        in_specs=[vmem()],
        out_specs=vmem(),
        compiler_params=pltpu.CompilerParams(vmem_limit_bytes=8 * MIB),
        name="reduce_pieces",
    )(pieces)


def direction_of(proj, m_one, m_two, inverse):
    normed = proj * inverse
    first = beta_one * m_one + (1 - beta_one) * normed
    second = beta_two * m_two + (1 - beta_two) * normed * normed
    return first, second, (first * lax.rsqrt(second)).astype(jnp.bfloat16)


def offsets(core):
    return (0, 3 - 2 * core, 1 + 2 * core, 2)


def finish_kernel(*refs):
    place_ref, pieces_ref = refs[:2]
    p_refs = refs[2:4]
    wm_refs = (refs[4:8], refs[8:12])
    p_own_refs = refs[12:15]
    m_refs = refs[15:18]
    step_refs = refs[18:21]
    copy_refs = refs[21:24]
    new_m_refs = refs[24:27]
    proj_ref, dir_ref, p_buf, wm_buf, p_own_buf, m_buf, turn_buf = refs[27:34]
    out_bufs = refs[34:37]
    p_sem, wm_sem, small_sem, out_sem = refs[37:]
    z, y, core = place_ref[0], place_ref[1], place_ref[2]
    slots = (core, 1 - core)
    mine = (z * 4 + y) * 2 + core
    levels = [[lax.rem(z + d, 4) for d in offsets(slot)] for slot in slots]
    columns = [[lax.rem(y + d, 4) for d in offsets(slot)] for slot in slots]

    wm_copies = []
    p_copies = []
    for array in range(4):
        for side in range(2):
            copy = pltpu.make_async_copy(
                wm_refs[side][array],
                wm_buf.at[side, pl.ds(4 * array, 4)],
                wm_sem.at[array * 2 + side],
            )
            copy.start()
            wm_copies.append(copy)
    small = []
    for member in range(3):
        for refs_of, buf, sem in ((m_refs, m_buf, member), (p_own_refs, p_own_buf, 3 + member)):
            copy = pltpu.make_async_copy(refs_of[member], buf.at[member], small_sem.at[sem])
            copy.start()
            small.append(copy)
    for array in range(4):
        for side in range(2):
            for index in range(4):
                spot = array * 4 + index
                place = levels[side][array] * 4 + columns[side][index]
                copy = pltpu.make_async_copy(
                    p_refs[side].at[place], p_buf.at[side, spot], p_sem.at[side * 16 + spot]
                )
                copy.start()
                p_copies.append(copy)

    squares = jnp.zeros((8, 128), jnp.float32)
    upper = lax.broadcasted_iota(jnp.int32, (32, 8, 128), 1) < 4
    for half in range(2):
        one = pieces_ref[:, 2 * half].astype(jnp.float32)
        two = pieces_ref[:, 2 * half + 1].astype(jnp.float32)
        tails = jnp.where(upper, 0.0, one[:, 8:] + two[:, 8:])
        squares = squares + jnp.sum(tails, axis=0)
        shared = jnp.where(upper, one[:, 8:], pltpu.roll(two[:, 8:], 4, 1))
        for tile, value in enumerate((one[:, :8], two[:, :8], shared)):
            proj_ref[:, :, pl.ds((3 * half + tile) * 128, 128)] = value
    total = jnp.sum(squares)
    inverse = lax.rsqrt(jnp.full((8, 768), total / 786432 + 1e-06))

    for array in range(4):
        for side in range(2):
            wm_copies[array * 2 + side].wait()
            for index in range(4):
                spot = array * 4 + index
                row = (levels[side][array] * 4 + columns[side][index]) * 2 + slots[side]
                dir_ref[row] = direction_of(
                    proj_ref[row],
                    wm_buf[side, spot, 64:72].astype(jnp.float32),
                    wm_buf[side, spot, 72:80].astype(jnp.float32),
                    inverse,
                )[2].astype(jnp.float32)

    directions = []
    for member in range(3):
        cols = pl.ds(member * 256, 256)
        directions.append(dir_ref[:, :, cols].reshape(256, 256).astype(jnp.bfloat16))
    outs = []
    for array in range(4):
        for side in range(2):
            for copy in p_copies[(array * 2 + side) * 4 :][:4]:
                copy.wait()
            spots = pl.ds(array * 4, 4)
            for member in range(3):
                cols = pl.ds(member * 256, 256)
                step = jnp.dot(
                    p_buf[side, spots, :, cols].reshape(256, 256),
                    directions[member],
                    preferred_element_type=jnp.float32,
                ).reshape(4, 64, 256)
                weight = wm_buf[side, spots, :64, cols].astype(jnp.float32)
                fresh = (weight - learn_rate * step).astype(jnp.bfloat16)
                target = out_bufs[member] if member < 2 else turn_buf
                for index in range(4):
                    place = levels[side][array] * 4 + columns[side][index]
                    target[place, slots[side]] = fresh[index]
                if member < 2:
                    part = pl.ds(levels[side][array] * 4, 4)
                    copy = pltpu.make_async_copy(
                        out_bufs[member].at[part, slots[side]],
                        copy_refs[member].at[part, slots[side]],
                        out_sem.at[(array * 2 + side) * 2 + member],
                    )
                    copy.start()
                    outs.append(copy)
        if array == 1:
            continue
        for done in (1, 2) if array == 2 else (array,):
            level = levels[0][done]
            for index in range(4):
                place = level * 4 + index
                lanes = pl.ds(pl.multiple_of(place * 128, 128), 128)
                out_bufs[2][:, lanes] = turn_buf[place].reshape(128, 256).T
            part = pl.ds(pl.multiple_of(level * 512, 512), 512)
            copy = pltpu.make_async_copy(
                out_bufs[2].at[:, part], copy_refs[2].at[:, part], out_sem.at[16 + done]
            )
            copy.start()
            outs.append(copy)

    for copy in small:
        copy.wait()
    for member in range(3):
        cols = pl.ds(member * 256, 256)
        first, second, _ = direction_of(
            proj_ref[mine, :, cols], m_buf[member, 0], m_buf[member, 1], inverse[:, :256]
        )
        new_m_refs[member][0] = first
        new_m_refs[member][1] = second
        step_refs[member][...] = jnp.dot(
            p_own_buf[member], directions[member], preferred_element_type=jnp.float32
        )
    for copy in outs:
        copy.wait()


def finish(place, pieces, p_a, p_b, wm_a, wm_b, p_own, moments):
    rows = pltpu.HBM((16, 2, 64, 256), jnp.bfloat16)
    turned = pltpu.HBM((256, 2048), jnp.bfloat16)
    step = jax.ShapeDtypeStruct((64, 256), jnp.float32)
    moment = jax.ShapeDtypeStruct((2, 8, 256), jnp.float32)
    fetched = [hbm_only(a) for a in (p_a, p_b, *wm_a, *wm_b, *p_own, *moments)]
    return pl.pallas_call(
        finish_kernel,
        out_shape=(step,) * 3 + (rows, rows, turned) + (moment,) * 3,
        in_specs=[smem(), vmem()] + [in_hbm()] * len(fetched),
        out_specs=(vmem(),) * 3 + (in_hbm(),) * 3 + (vmem(),) * 3,
        scratch_shapes=[
            pltpu.VMEM((32, 8, 768), jnp.float32),
            pltpu.VMEM((32, 8, 768), jnp.float32),
            pltpu.VMEM((2, 16, 64, 768), jnp.bfloat16),
            pltpu.VMEM((2, 16, 80, 768), jnp.bfloat16),
            pltpu.VMEM((3, 64, 256), jnp.bfloat16),
            pltpu.VMEM((3, 2, 8, 256), jnp.float32),
            pltpu.VMEM((16, 2, 64, 256), jnp.bfloat16),
            pltpu.VMEM((16, 2, 64, 256), jnp.bfloat16),
            pltpu.VMEM((16, 2, 64, 256), jnp.bfloat16),
            pltpu.VMEM((256, 2048), jnp.bfloat16),
            pltpu.SemaphoreType.DMA((32,)),
            pltpu.SemaphoreType.DMA((8,)),
            pltpu.SemaphoreType.DMA((6,)),
            pltpu.SemaphoreType.DMA((20,)),
        ],
        compiler_params=pltpu.CompilerParams(vmem_limit_bytes=32 * MIB),
        name="finish",
    )(place, pieces, *fetched)


def body(
    x_saved,
    h_saved,
    key_cot,
    value_cot,
    out_cot,
    w_key,
    w_value,
    w_out,
    p_key,
    p_value,
    p_out,
    m_key,
    m_value,
    m_out,
):
    place = jnp.stack([lax.axis_index(a) for a in FS]).astype(jnp.int32)
    core = place[2:]
    p_all = spread(p_key, p_value, p_out)
    p_a = lax.all_to_all(p_all, FAR, 0, 0, tiled=True)

    keep, send = grad_halves(core, key_cot, value_cot, h_saved, x_saved, out_cot)
    recv = swap(send)

    w_own = jnp.concatenate([w_key, w_value, w_out.T], axis=1)
    m_own = jnp.concatenate([m_key, m_value, m_out], axis=2).reshape(16, 768)
    wm_own = jnp.concatenate([w_own, m_own], axis=0).astype(jnp.bfloat16)
    wm_y = [wm_own] + [mirrored(wm_own, "fs_1", by) for by in (1, -1, 2)]
    wm_y = jnp.stack(wm_y)

    parts = pair_sum(keep, recv)
    partial = project(parts, p_a.reshape(1024, 768))
    pieces = lax.all_to_all(
        partial.reshape(128, 16, 128), (*FS, "tp"), 0, 0, tiled=True
    )
    wm_near = mirrored(wm_y, "fs_0", 1)
    wm_next = mirrored(wm_y, "fs_0", -1)
    p_b = swap(p_a)

    packed = reduce_pieces(pieces.reshape(32, 4, 16, 128))
    whole = lax.all_to_all(packed.reshape(128, 16, 128), (*FS, "tp"), 0, 0, tiled=True)
    wm_far = mirrored(wm_near, "fs_0", 1)
    wm_a = (wm_y, wm_near, wm_next, wm_far)
    wm_b = tuple(swap(a) for a in wm_a)
    outs = finish(
        place,
        whole.reshape(32, 4, 16, 128),
        p_a,
        p_b,
        wm_a,
        wm_b,
        (p_key, p_value, p_out),
        (m_key, m_value, m_out),
    )
    return (
        outs[0],
        outs[1],
        outs[2].T,
        outs[3].reshape(2048, 256),
        outs[4].reshape(2048, 256),
        *outs[5:],
    )


def solution(mesh):
    split = Mesh(mesh.devices.reshape(4, 4, 2, mesh.shape["tp"]), ("fs_0", "fs_1", "fs_2", "tp"))
    in_specs = (
        P(FS, None),
        P(FS, "tp"),
        P(FS, "tp"),
        P(FS, "tp"),
        P(FS, None),
        P(FS, "tp"),
        P(FS, "tp"),
        P("tp", FS),
        P(FS, None),
        P(FS, None),
        P(FS, None),
        P(None, FS, "tp"),
        P(None, FS, "tp"),
        P(None, FS, "tp"),
    )
    out_specs = (
        P(FS, "tp"),
        P(FS, "tp"),
        P("tp", FS),
        P(None, "tp"),
        P(None, "tp"),
        P("tp", None),
        P(None, FS, "tp"),
        P(None, FS, "tp"),
        P(None, FS, "tp"),
    )
    return jax.shard_map(
        body, mesh=split, in_specs=in_specs, out_specs=out_specs, check_vma=False
    )
```

time: 156 us -> 94.8 us (0.61)
  blocking collectives: 44.8 us -> 0 us
  Pallas kernels: 0 us -> 27.1 us
  matrix products: 19.4 us -> 0 us
  waiting for transfers between devices: 43.5 us -> 27.8 us
  local copies, waits for them, and re-layouts: 13.8 us -> 0.05 us
  starting transfers between devices: 23.2 us -> 36.5 us
  other arithmetic: 8.29 us -> 1.95 us
    all_to_all x5 -> x0, blocking collectives: 44.8 us -> none  [copy_for_each(): return lax.all_to_all(copies, axis, split_axis=0, concat_axis=0, tiled=True)]
    pallas_call x0 -> x6, Pallas kernels: none -> 27.1 us  [the longest x1 11.8 us: grad_halves(): pl.pallas_call(grad_kernel, out_shape=(pltpu.HBM((768, 1024), jnp.float32...]
    dot_general x12 -> x0, matrix products: 19.4 us -> none  [the longest x1 5.9 us: body(): grad_k = jnp.dot(x_cols, key_cot, preferred_element_type=jnp.float32)]
    all_to_all x5 -> x3, waiting for transfers between devices: 43.5 us -> 24.5 us  [the longest x1 10.5 us: body(): lax.all_to_all(partial.reshape(128, 16, 128), (*FS, 'tp'), 0, 0, tiled=True)]
    ppermute x0 -> x12, starting transfers between devices: none -> 16.8 us  [the longest x6 9.96 us: mirrored(): return lax.ppermute(value, (axis, CORE), pairs)]
    broadcast_in_dim x9 -> x0, local copies, waits for them, and re-layouts: 5.9 us -> none  [copy_for_each(): copies = jnp.broadcast_to(value, (lax.axis_size(axis), *value.shape))]
    unnamed x35 -> x18, local copies, waits for them, and re-layouts: 4.84 us -> 0.05 us
    convert_element_type x3 -> x0, other arithmetic: 4.09 us -> none  [the longest x1 2.08 us: project_rows(): low_part = (grads - high_part.astype(jnp.float32)).astype(jnp.bfloat16)]
  transfers between devices with their start and end apart: 5 -> 15, of which waited for: 5 -> 8; matrix products, arithmetic and copies ran while one was open for 15% -> 2% of each run, Pallas kernels for 0% -> 17%
where the time goes in v1:
time: 94.8 us; the launch traced here: 94.4 us
  starting transfers between devices  36.5 us (39%)
  waiting for transfers between devices  27.8 us (29%)
  Pallas kernels  27.1 us (29%)
  other arithmetic  1.95 us (2%)
  between operations  0.97 us (1%)
    pallas_call x1, Pallas kernels, grad_halves(): pl.pallas_call(grad_kernel, out_shape=(pltpu.HBM((768, 1024), jnp.float32...  11.8 us
    all_to_all x1, waiting for transfers between devices, body(): lax.all_to_all(partial.reshape(128, 16, 128), (*FS, 'tp'), 0, 0, tiled=True)  10.5 us
    ppermute x6, starting transfers between devices, mirrored(): return lax.ppermute(value, (axis, CORE), pairs)  9.96 us
    pallas_call x1, Pallas kernels, finish(): pl.pallas_call(finish_kernel, out_shape=(step,) * 3 + (rows, rows, turned...  8.75 us
    all_to_all x1, waiting for transfers between devices, body(): lax.all_to_all(packed.reshape(128, 16, 128), (*FS, 'tp'), 0, 0, tiled=True)  8.64 us
    all_to_all x1, starting transfers between devices, body(): p_a = lax.all_to_all(p_all, FAR, 0, 0, tiled=True)  8.59 us
    all_to_all x1, starting transfers between devices, body(): lax.all_to_all(partial.reshape(128, 16, 128), (*FS, 'tp'), 0, 0, tiled=True)  7.28 us
    ppermute x6, starting transfers between devices, shift(): lax.ppermute(value, axis, [(i, (i + by) % size) for i in range(size)])  6.84 us
  transfers between devices with their start and end apart: 15, of which 8 were waited for; matrix products, arithmetic and copies ran while one was open for 2% of the time, Pallas kernels for 17%

profile of v1, /device:TPU:1, one launch (start us, length us, event | category | flops | bytes accessed | tf_op | source)
XLA Modules:
  0.0 94.4 jit_solution(9937417715533794821)
XLA Ops:
  0.6 2.1 %spread.1 = bf16[16,64,768]{2,1,0:T(8,128)(2,1)} custom-call(bf16[64,256]{1,0:T(8,128)(2,1)} %refs_12_.1, bf16[64,256]{1,0:T(8,128)(2,1)} %refs_13_.1, bf16[64,256]{1,0:T(8,128)(2,1)} %refs_14_.1), custom_call_target="tpu_custom_call" | custom-call | tf_op jit(solution)/shard_map/spread/pallas_call | solution.py:52
  2.7 8.6 %all-to-all-start = ((bf16[16,64,768]{2,1,0:T(8,128)(2,1)}), bf16[16,64,768]{2,1,0:T(8,128)(2,1)S(1)}, u32[]{:S(2)}, u32[]{:S(2)}) async-start(bf16[16,64,768]{2,1,0:T(8,128)(2,1)} %spread.1), calls=%async_computation | async-start | bytes 3145728 | tf_op jit(solution)/shard_map/all_to_all | solution.py:456
  11.3 0.0 copy-start.6
  11.3 0.0 copy-start.7
  11.3 0.0 copy-start.8
  11.4 0.0 copy-start.3
  11.4 0.0 copy-start.4
  11.4 0.0 copy-start.5
  11.4 11.8 %grads.1 = (f32[768,1024]{1,0:T(8,128)}, bf16[768,1024]{1,0:T(8,128)(2,1)}) custom-call(s32[1]{0:T(128)} %bitcast.2.core_ref, bf16[2048,256]{1,0:T(8,128)(2,1)} %k_ref.1, bf16[2048,256]{1,0:T(8,128)(2,1)} %v_ref.1, bf16[2048,256]{1,0:T(8,128)(2,1)} %h_ref.1, bf16[2048,2048]{1,0:T(8,128)(2,1)} %x_ref.1, bf16[2048,2048]{1,0:T(8,128)(2,1)} %o_ref.1), custom_call_target="tpu_custom_call" | custom-call | tf_op jit(solution)/shard_map/grads/pallas_call | solution.py:154
  23.2 1.0 %collective-permute-start = (bf16[768,1024]{1,0:T(8,128)(2,1)}, bf16[768,1024]{1,0:T(8,128)(2,1)S(1)}, u32[]{:S(2)}, u32[]{:S(2)}) collective-permute-start(bf16[768,1024]{1,0:T(8,128)(2,1)} %get-tuple-element.21), channel_id=1, source_target_pairs={{0,4},{4,0},{1,5},{5,1},{2,6},{6,2},{3,7},{7,3},{8,12},{12,8},{9,1... | collective-permute-start | bytes 4718600 | tf_op jit(solution)/shard_map/ppermute | solution.py:29
  24.3 0.0 copy-done.6
  24.3 0.0 copy-done.7
  24.3 0.0 copy-done.8
  24.3 0.0 copy-done.3
  24.3 0.0 copy-done.4
  24.3 0.0 copy-done.5
  24.4 2.9 %collective-permute-start.2 = (bf16[80,768]{1,0:T(8,128)(2,1)S(1)}, bf16[80,768]{1,0:T(8,128)(2,1)S(1)}, u32[]{:S(2)}, u32[]{:S(2)}) collective-permute-start(bf16[80,768]{1,0:T(8,128)(2,1)S(1)} %pad_maximum_fusion.1), channel_id=1, source_target_pairs={{0,8},{4,28},{8,16},{12,4},{16,24},{20,12},{24,0},{28,20},{1,9},{5... | collective-permute-start | bytes 368648 | tf_op jit(solution)/shard_map/ppermute | solution.py:38
  27.3 0.0 collective-permute-start.3
  27.3 1.7 %collective-permute-start.4 = (bf16[80,768]{1,0:T(8,128)(2,1)S(1)}, bf16[80,768]{1,0:T(8,128)(2,1)}, u32[]{:S(2)}, u32[]{:S(2)}) collective-permute-start(bf16[80,768]{1,0:T(8,128)(2,1)S(1)} %pad_maximum_fusion.1), channel_id=1, source_target_pairs={{0,16},{4,20},{8,24},{12,28},{16,0},{20,4},{24,8},{28,12},{1,17},{... | collective-permute-start | bytes 368648 | tf_op jit(solution)/shard_map/ppermute | solution.py:38
  29.0 5.4 %all-to-all-done.refs_2_ = bf16[16,64,768]{2,1,0:T(8,128)(2,1)S(1)} async-done(((bf16[16,64,768]{2,1,0:T(8,128)(2,1)}), bf16[16,64,768]{2,1,0:T(8,128)(2,1)S(1)}, u32[]{:S(2)}, u32[]{:S(2)}) %all-to-all-start) | async-done | bytes 1572896 | tf_op jit(solution)/shard_map/all_to_all | solution.py:456
  34.4 0.0 copy-start
  34.4 3.6 %collective-permute-start.1 = (bf16[16,64,768]{2,1,0:T(8,128)(2,1)S(1)}, bf16[16,64,768]{2,1,0:T(8,128)(2,1)}, u32[]{:S(2)}, u32[]{:S(2)}) collective-permute-start(bf16[16,64,768]{2,1,0:T(8,128)(2,1)S(1)} %all-to-all-done.refs_2_), channel_id=1, source_target_pairs={{0,4},{4,0},{1,5},{5,1},{2,6},{6,2},{3,7},{7,3},{8,12},{12,8},{9,1... | collective-permute-start | bytes 4718600 | tf_op jit(solution)/shard_map/ppermute | solution.py:29
  38.0 0.0 collective-permute-done.2
  38.0 0.0 collective-permute-done.3
  38.0 0.2 collective-permute-done.4
  38.2 1.8 %pad_maximum_fusion.refs_4_ = bf16[4,80,768]{2,1,0:T(8,128)(2,1)} fusion(bf16[1,80,768]{2,1,0:T(8,128)(2,1)} %bitcast.14, bf16[1,80,768]{2,1,0:T(8,128)(2,1)} %bitcast.13, bf16[1,80,768]{2,1,0:T(8,128)(2,1)S(1)} %bitcast.26, bf16[1,16,768]{2,1,0:T(8,128)(2,1)S(1)} %get-tuple-element.31, bf16[1,64,768]{2,1,0:T(8,128)(2,1)S(1)} %fusion.2), kind=kLoop, calls=%fused_computation | loop fusion | flops 2457600 | bytes 983040 | tf_op jit(solution)/shard_map/stack | solution.py:465
  40.0 1.9 %collective-permute-start.5 = (bf16[4,80,768]{2,1,0:T(8,128)(2,1)}, bf16[4,80,768]{2,1,0:T(8,128)(2,1)}, u32[]{:S(2)}, u32[]{:S(2)}) collective-permute-start(bf16[4,80,768]{2,1,0:T(8,128)(2,1)} %pad_maximum_fusion.refs_4_), channel_id=1, source_target_pairs={{0,32},{4,100},{32,64},{36,4},{64,96},{68,36},{96,0},{100,68},{1,3... | collective-permute-start | bytes 1474568 | tf_op jit(solution)/shard_map/ppermute | solution.py:38
  41.9 0.0 collective-permute-done.recv_ref
  42.0 2.0 %pair_sum.1.parts_ref = bf16[3,256,1024]{2,1,0:T(8,128)(2,1)S(1)} custom-call(f32[768,1024]{1,0:T(8,128)} %get-tuple-element.20.keep_ref, bf16[768,1024]{1,0:T(8,128)(2,1)S(1)} %collective-permute-done.recv_ref), custom_call_target="tpu_custom_call" | custom-call | tf_op jit(solution)/shard_map/pair_sum/pallas_call | solution.py:192
  43.9 0.0 copy-done
  43.9 1.5 %project.1 = bf16[32,4,16,128]{3,2,1,0:T(8,128)(2,1)} custom-call(bf16[3,256,1024]{2,1,0:T(8,128)(2,1)S(1)} %pair_sum.1.parts_ref, bf16[1024,768]{1,0:T(8,128)(2,1)S(1)} %bitcast.21), custom_call_target="tpu_custom_call" | custom-call | tf_op jit(solution)/shard_map/project/pallas_call | solution.py:227
  45.4 7.3 %all-to-all-start.1 = ((bf16[128,16,128]{2,1,0:T(8,128)(2,1)}), bf16[128,16,128]{2,1,0:T(8,128)(2,1)S(1)}, u32[]{:S(2)}, u32[]{:S(2)}) async-start(bf16[128,16,128]{2,1,0:T(8,128)(2,1)} %bitcast.4), calls=%async_computation.1 | async-start | bytes 1048576 | tf_op jit(solution)/shard_map/all_to_all | solution.py:469
  52.7 1.6 %collective-permute-start.6 = (bf16[4,80,768]{2,1,0:T(8,128)(2,1)}, bf16[4,80,768]{2,1,0:T(8,128)(2,1)S(1)}, u32[]{:S(2)}, u32[]{:S(2)}) collective-permute-start(bf16[4,80,768]{2,1,0:T(8,128)(2,1)} %pad_maximum_fusion.refs_4_), channel_id=1, source_target_pairs={{0,96},{4,36},{32,0},{36,68},{64,32},{68,100},{96,64},{100,4},{1,9... | collective-permute-start | bytes 1474568 | tf_op jit(solution)/shard_map/ppermute | solution.py:38
  54.3 0.0 collective-permute-done.5.refs_5_
  54.3 1.8 %collective-permute-start.7 = (bf16[4,80,768]{2,1,0:T(8,128)(2,1)}, bf16[4,80,768]{2,1,0:T(8,128)(2,1)S(1)}, u32[]{:S(2)}, u32[]{:S(2)}) collective-permute-start(bf16[4,80,768]{2,1,0:T(8,128)(2,1)} %collective-permute-done.5.refs_5_), channel_id=1, source_target_pairs={{0,32},{4,100},{32,64},{36,4},{64,96},{68,36},{96,0},{100,68},{1,3... | collective-permute-start | bytes 1474568 | tf_op jit(solution)/shard_map/ppermute | solution.py:38
  56.1 10.5 %all-to-all-done.1 = bf16[128,16,128]{2,1,0:T(8,128)(2,1)S(1)} async-done(((bf16[128,16,128]{2,1,0:T(8,128)(2,1)}), bf16[128,16,128]{2,1,0:T(8,128)(2,1)S(1)}, u32[]{:S(2)}, u32[]{:S(2)}) %all-to-all-start.1) | async-done | bytes 524320 | tf_op jit(solution)/shard_map/all_to_all | solution.py:469
  66.6 1.1 %reduce_pieces.1 = bf16[32,4,16,128]{3,2,1,0:T(8,128)(2,1)} custom-call(bf16[32,4,16,128]{3,2,1,0:T(8,128)(2,1)S(1)} %bitcast.22), custom_call_target="tpu_custom_call" | custom-call | tf_op jit(solution)/shard_map/reduce_pieces/pallas_call | solution.py:249
  67.7 3.9 %all-to-all-start.2 = ((bf16[128,16,128]{2,1,0:T(8,128)(2,1)}), bf16[128,16,128]{2,1,0:T(8,128)(2,1)S(1)}, u32[]{:S(2)}, u32[]{:S(2)}) async-start(bf16[128,16,128]{2,1,0:T(8,128)(2,1)} %bitcast.6), calls=%async_computation.2 | async-start | bytes 1048576 | tf_op jit(solution)/shard_map/all_to_all | solution.py:477
  71.5 1.4 %collective-permute-start.8 = (bf16[4,80,768]{2,1,0:T(8,128)(2,1)}, bf16[4,80,768]{2,1,0:T(8,128)(2,1)}, u32[]{:S(2)}, u32[]{:S(2)}) collective-permute-start(bf16[4,80,768]{2,1,0:T(8,128)(2,1)} %pad_maximum_fusion.refs_4_), channel_id=1, source_target_pairs={{0,4},{4,0},{1,5},{5,1},{2,6},{6,2},{3,7},{7,3},{8,12},{12,8},{9,1... | collective-permute-start | bytes 1474568 | tf_op jit(solution)/shard_map/ppermute | solution.py:29
  72.9 0.1 collective-permute-start.9
  73.0 0.0 collective-permute-done.6.refs_6_
  73.0 0.0 copy-start.1
  73.0 0.4 collective-permute-start.10
  73.5 0.0 collective-permute-done.7.refs_7_
  73.5 0.0 copy-start.2
  73.5 0.3 collective-permute-start.11
  73.7 0.1 pad_add_fusion.refs_0_
  73.8 0.9 %collective-permute-done.8.refs_8_ = bf16[4,80,768]{2,1,0:T(8,128)(2,1)} collective-permute-done((bf16[4,80,768]{2,1,0:T(8,128)(2,1)}, bf16[4,80,768]{2,1,0:T(8,128)(2,1)}, u32[]{:S(2)}, u32[]{:S(2)}) %collective-permute-start.8) | collective-permute-done | bytes 491552 | tf_op jit(solution)/shard_map/ppermute | solution.py:29
  74.8 0.7 collective-permute-done.9.refs_9_
  75.5 0.7 collective-permute-done.10.refs_10_
  76.2 0.7 collective-permute-done.11.refs_11_
  76.9 8.6 %all-to-all-done.2 = bf16[128,16,128]{2,1,0:T(8,128)(2,1)S(1)} async-done(((bf16[128,16,128]{2,1,0:T(8,128)(2,1)}), bf16[128,16,128]{2,1,0:T(8,128)(2,1)S(1)}, u32[]{:S(2)}, u32[]{:S(2)}) %all-to-all-start.2) | async-done | bytes 524320 | tf_op jit(solution)/shard_map/all_to_all | solution.py:477
  85.5 0.0 collective-permute-done.1.refs_3_
  85.5 0.0 copy-done.1
  85.5 0.0 copy-done.2
  85.5 8.7 %finish.1 = (f32[64,256]{1,0:T(8,128)}, f32[64,256]{1,0:T(8,128)}, f32[64,256]{1,0:T(8,128)}, bf16[16,2,64,256]{3,2,1,0:T(8,128)(2,1)}, bf16[16,2,64,256]{3,2,1,...) custom-call(s32[3]{0:T(128)S(1)} %pad_add_fusion.refs_0_, ...), custom_call_target="tpu_custom_call" | custom-call | tf_op jit(solution)/shard_map/finish/pallas_call | solution.py:411
  (4 shorter events, 0.0 us)
Async XLA Ops:
  2.7 31.7 %all-to-all-start = ((bf16[16,64,768]{2,1,0:T(8,128)(2,1)}), bf16[16,64,768]{2,1,0:T(8,128)(2,1)S(1)}, u32[]{:S(2)}, u32[]{:S(2)}) async-start(bf16[16,64,768]{2,1,0:T(8,128)(2,1)} %spread.1), calls=%async_computation | async-start | bytes 3145728 | tf_op jit(solution)/shard_map/all_to_all | solution.py:456
  11.3 12.9 %copy-start.6 = (f32[2,8,256]{2,1,0:T(8,128)S(1)}, f32[2,8,256]{2,1,0:T(8,128)}, u32[]{:S(2)}) copy-start(f32[2,8,256]{2,1,0:T(8,128)} %refs_17_.1) | copy-start | bytes 49156
  11.3 12.9 %copy-start.7 = (f32[2,8,256]{2,1,0:T(8,128)S(1)}, f32[2,8,256]{2,1,0:T(8,128)}, u32[]{:S(2)}) copy-start(f32[2,8,256]{2,1,0:T(8,128)} %refs_16_.1) | copy-start | bytes 49156
  11.3 12.9 %copy-start.8 = (f32[2,8,256]{2,1,0:T(8,128)S(1)}, f32[2,8,256]{2,1,0:T(8,128)}, u32[]{:S(2)}) copy-start(f32[2,8,256]{2,1,0:T(8,128)} %refs_15_.1) | copy-start | bytes 49156
  11.4 12.9 %copy-start.3 = (f32[256,64]{0,1:T(8,128)S(1)}, f32[256,64]{0,1:T(8,128)}, u32[]{:S(2)}) copy-start(f32[256,64]{0,1:T(8,128)} %param.21) | copy-start | bytes 196612
  11.4 12.9 %copy-start.4 = (f32[64,256]{1,0:T(8,128)S(1)}, f32[64,256]{1,0:T(8,128)}, u32[]{:S(2)}) copy-start(f32[64,256]{1,0:T(8,128)} %param.20) | copy-start | bytes 196612
  11.4 12.9 %copy-start.5 = (f32[64,256]{1,0:T(8,128)S(1)}, f32[64,256]{1,0:T(8,128)}, u32[]{:S(2)}) copy-start(f32[64,256]{1,0:T(8,128)} %param.19) | copy-start | bytes 196612
  23.2 18.7 %collective-permute-start = (bf16[768,1024]{1,0:T(8,128)(2,1)}, bf16[768,1024]{1,0:T(8,128)(2,1)S(1)}, u32[]{:S(2)}, u32[]{:S(2)}) collective-permute-start(bf16[768,1024]{1,0:T(8,128)(2,1)} %get-tuple-element.21), channel_id=1, source_target_pairs={{0,4},{4,0},{1,5},{5,1},{2,6},{6,2},{3,7},{7,3},{8,12},{12,8},{9,1... | collective-permute-start | bytes 4718600 | tf_op jit(solution)/shard_map/ppermute | solution.py:29
  24.4 13.7 %collective-permute-start.2 = (bf16[80,768]{1,0:T(8,128)(2,1)S(1)}, bf16[80,768]{1,0:T(8,128)(2,1)S(1)}, u32[]{:S(2)}, u32[]{:S(2)}) collective-permute-start(bf16[80,768]{1,0:T(8,128)(2,1)S(1)} %pad_maximum_fusion.1), channel_id=1, source_target_pairs={{0,8},{4,28},{8,16},{12,4},{16,24},{20,12},{24,0},{28,20},{1,9},{5... | collective-permute-start | bytes 368648 | tf_op jit(solution)/shard_map/ppermute | solution.py:38
  27.3 10.7 %collective-permute-start.3 = (bf16[80,768]{1,0:T(8,128)(2,1)S(1)}, bf16[80,768]{1,0:T(8,128)(2,1)}, u32[]{:S(2)}, u32[]{:S(2)}) collective-permute-start(bf16[80,768]{1,0:T(8,128)(2,1)S(1)} %pad_maximum_fusion.1), channel_id=1, source_target_pairs={{0,24},{4,12},{8,0},{12,20},{16,8},{20,28},{24,16},{28,4},{1,25},{... | collective-permute-start | bytes 368648 | tf_op jit(solution)/shard_map/ppermute | solution.py:38
  27.3 10.9 %collective-permute-start.4 = (bf16[80,768]{1,0:T(8,128)(2,1)S(1)}, bf16[80,768]{1,0:T(8,128)(2,1)}, u32[]{:S(2)}, u32[]{:S(2)}) collective-permute-start(bf16[80,768]{1,0:T(8,128)(2,1)S(1)} %pad_maximum_fusion.1), channel_id=1, source_target_pairs={{0,16},{4,20},{8,24},{12,28},{16,0},{20,4},{24,8},{28,12},{1,17},{... | collective-permute-start | bytes 368648 | tf_op jit(solution)/shard_map/ppermute | solution.py:38
  34.4 9.5 %copy-start = (bf16[16,64,768]{2,1,0:T(8,128)(2,1)}, bf16[16,64,768]{2,1,0:T(8,128)(2,1)S(1)}, u32[]{:S(2)}) copy-start(bf16[16,64,768]{2,1,0:T(8,128)(2,1)S(1)} %all-to-all-done.refs_2_) | copy-start | bytes 4718596
  34.4 51.1 %collective-permute-start.1 = (bf16[16,64,768]{2,1,0:T(8,128)(2,1)S(1)}, bf16[16,64,768]{2,1,0:T(8,128)(2,1)}, u32[]{:S(2)}, u32[]{:S(2)}) collective-permute-start(bf16[16,64,768]{2,1,0:T(8,128)(2,1)S(1)} %all-to-all-done.refs_2_), channel_id=1, source_target_pairs={{0,4},{4,0},{1,5},{5,1},{2,6},{6,2},{3,7},{7,3},{8,12},{12,8},{9,1... | collective-permute-start | bytes 4718600 | tf_op jit(solution)/shard_map/ppermute | solution.py:29
  40.0 14.2 %collective-permute-start.5 = (bf16[4,80,768]{2,1,0:T(8,128)(2,1)}, bf16[4,80,768]{2,1,0:T(8,128)(2,1)}, u32[]{:S(2)}, u32[]{:S(2)}) collective-permute-start(bf16[4,80,768]{2,1,0:T(8,128)(2,1)} %pad_maximum_fusion.refs_4_), channel_id=1, source_target_pairs={{0,32},{4,100},{32,64},{36,4},{64,96},{68,36},{96,0},{100,68},{1,3... | collective-permute-start | bytes 1474568 | tf_op jit(solution)/shard_map/ppermute | solution.py:38
  45.4 21.2 %all-to-all-start.1 = ((bf16[128,16,128]{2,1,0:T(8,128)(2,1)}), bf16[128,16,128]{2,1,0:T(8,128)(2,1)S(1)}, u32[]{:S(2)}, u32[]{:S(2)}) async-start(bf16[128,16,128]{2,1,0:T(8,128)(2,1)} %bitcast.4), calls=%async_computation.1 | async-start | bytes 1048576 | tf_op jit(solution)/shard_map/all_to_all | solution.py:469
  52.7 20.3 %collective-permute-start.6 = (bf16[4,80,768]{2,1,0:T(8,128)(2,1)}, bf16[4,80,768]{2,1,0:T(8,128)(2,1)S(1)}, u32[]{:S(2)}, u32[]{:S(2)}) collective-permute-start(bf16[4,80,768]{2,1,0:T(8,128)(2,1)} %pad_maximum_fusion.refs_4_), channel_id=1, source_target_pairs={{0,96},{4,36},{32,0},{36,68},{64,32},{68,100},{96,64},{100,4},{1,9... | collective-permute-start | bytes 1474568 | tf_op jit(solution)/shard_map/ppermute | solution.py:38
  54.3 19.2 %collective-permute-start.7 = (bf16[4,80,768]{2,1,0:T(8,128)(2,1)}, bf16[4,80,768]{2,1,0:T(8,128)(2,1)S(1)}, u32[]{:S(2)}, u32[]{:S(2)}) collective-permute-start(bf16[4,80,768]{2,1,0:T(8,128)(2,1)} %collective-permute-done.5.refs_5_), channel_id=1, source_target_pairs={{0,32},{4,100},{32,64},{36,4},{64,96},{68,36},{96,0},{100,68},{1,3... | collective-permute-start | bytes 1474568 | tf_op jit(solution)/shard_map/ppermute | solution.py:38
  67.7 17.9 %all-to-all-start.2 = ((bf16[128,16,128]{2,1,0:T(8,128)(2,1)}), bf16[128,16,128]{2,1,0:T(8,128)(2,1)S(1)}, u32[]{:S(2)}, u32[]{:S(2)}) async-start(bf16[128,16,128]{2,1,0:T(8,128)(2,1)} %bitcast.6), calls=%async_computation.2 | async-start | bytes 1048576 | tf_op jit(solution)/shard_map/all_to_all | solution.py:477
  71.5 3.2 %collective-permute-start.8 = (bf16[4,80,768]{2,1,0:T(8,128)(2,1)}, bf16[4,80,768]{2,1,0:T(8,128)(2,1)}, u32[]{:S(2)}, u32[]{:S(2)}) collective-permute-start(bf16[4,80,768]{2,1,0:T(8,128)(2,1)} %pad_maximum_fusion.refs_4_), channel_id=1, source_target_pairs={{0,4},{4,0},{1,5},{5,1},{2,6},{6,2},{3,7},{7,3},{8,12},{12,8},{9,1... | collective-permute-start | bytes 1474568 | tf_op jit(solution)/shard_map/ppermute | solution.py:29
  72.9 2.5 %collective-permute-start.9 = (bf16[4,80,768]{2,1,0:T(8,128)(2,1)}, bf16[4,80,768]{2,1,0:T(8,128)(2,1)}, u32[]{:S(2)}, u32[]{:S(2)}) collective-permute-start(bf16[4,80,768]{2,1,0:T(8,128)(2,1)} %collective-permute-done.5.refs_5_), channel_id=1, source_target_pairs={{0,4},{4,0},{1,5},{5,1},{2,6},{6,2},{3,7},{7,3},{8,12},{12,8},{9,1... | collective-permute-start | bytes 1474568 | tf_op jit(solution)/shard_map/ppermute | solution.py:29
  73.0 12.5 %copy-start.1 = (bf16[4,80,768]{2,1,0:T(8,128)(2,1)}, bf16[4,80,768]{2,1,0:T(8,128)(2,1)S(1)}, u32[]{:S(2)}) copy-start(bf16[4,80,768]{2,1,0:T(8,128)(2,1)S(1)} %collective-permute-done.6.refs_6_) | copy-start | bytes 1474564
  73.0 3.1 %collective-permute-start.10 = (bf16[4,80,768]{2,1,0:T(8,128)(2,1)S(1)}, bf16[4,80,768]{2,1,0:T(8,128)(2,1)}, u32[]{:S(2)}, u32[]{:S(2)}) collective-permute-start(bf16[4,80,768]{2,1,0:T(8,128)(2,1)S(1)} %collective-permute-done.6.refs_6_), channel_id=1, source_target_pairs={{0,4},{4,0},{1,5},{5,1},{2,6},{6,2},{3,7},{7,3},{8,12},{12,8},{9,1... | collective-permute-start | bytes 1474568 | tf_op jit(solution)/shard_map/ppermute | solution.py:29
  73.5 12.1 %copy-start.2 = (bf16[4,80,768]{2,1,0:T(8,128)(2,1)}, bf16[4,80,768]{2,1,0:T(8,128)(2,1)S(1)}, u32[]{:S(2)}) copy-start(bf16[4,80,768]{2,1,0:T(8,128)(2,1)S(1)} %collective-permute-done.7.refs_7_) | copy-start | bytes 1474564
  73.5 3.4 %collective-permute-start.11 = (bf16[4,80,768]{2,1,0:T(8,128)(2,1)S(1)}, bf16[4,80,768]{2,1,0:T(8,128)(2,1)}, u32[]{:S(2)}, u32[]{:S(2)}) collective-permute-start(bf16[4,80,768]{2,1,0:T(8,128)(2,1)S(1)} %collective-permute-done.7.refs_7_), channel_id=1, source_target_pairs={{0,4},{4,0},{1,5},{5,1},{2,6},{6,2},{3,7},{7,3},{8,12},{12,8},{9,1... | collective-permute-start | bytes 1474568 | tf_op jit(solution)/shard_map/ppermute | solution.py:29
